TPU v7x, 256 devices: a whole 4x4x8 slice. The times are simulated.
256 devices in a mesh: sp: 32 (over z, x), tp: 8 (over y, core).
Axes of the slice: x: 4, y: 4, z: 8, core: 2. Of those that a mesh axis runs over, the one named last changes fastest.
Arguments:
- resid: bfloat16 [8192, 4096], P('sp'), may hold values from -6 to 6
- queries: bfloat16 [8192, 3072], P('sp', 'tp'), may hold values from -1000 to 1000
- latent: bfloat16 [8192, 512], P('sp'), may hold values from -6 to 6
- rope_key: bfloat16 [8192, 64], P('sp'), may hold values from -6 to 6
- lat_gain: float32 [512], replicated, may hold values from 0.1 to 1.9
- kv_weight: bfloat16 [512, 4096], P(None, 'tp'), may hold values from -4 to 4
- out_gain: float32 [2048], P('tp'), may hold values from 0.1 to 1.9
- out_weight: bfloat16 [2048, 4096], P('tp'), may hold values from -0.125 to 0.125
- ffn_gain: float32 [4096], replicated, may hold values from 0.1 to 1.9
- gate_weight: bfloat16 [4096, 6144], P('sp', 'tp'), may hold values from -0.09375 to 0.09375
- up_weight: bfloat16 [4096, 6144], P('sp', 'tp'), may hold values from -0.09375 to 0.09375
- down_weight: bfloat16 [6144, 4096], P('tp', 'sp'), may hold values from -0.078125 to 0.078125
Outputs:
- result: bfloat16 [8192, 4096], P(('sp', 'tp'))
All inputs are finite; a program needn't handle non-finite values.
Results may differ from a plain program's by a relative error of at most 0.018.
Values may be sent and summed in bfloat16 or wider, within the bound.
A program may use at most 192 MiB of HBM per device.

v0:
```python
import math
import jax
import jax.numpy as jnp
from jax import lax
from jax.sharding import PartitionSpec as P

HEADS = 16
NOPE = 128
ROPE = 64
VDIM = 128
EPSILON = 1e-06
THETA = 10000.0
LOWEST = -1e30


def turned_gather(arrays, axis, dims):
    turned = [jnp.moveaxis(a, dim, 0) for a, dim in zip(arrays, dims)]
    both = jnp.concatenate([t.reshape(len(t), -1) for t in turned], axis=1)
    filled, at, outs = (lax.all_gather(both, axis, axis=0, tiled=True), 0, [])
    for t, dim in zip(turned, dims):
        slab = filled[:, at : at + t[0].size].reshape(-1, *t.shape[1:])
        outs.append(jnp.moveaxis(slab, 0, dim))
        at += t[0].size
    return tuple(outs)


def side_by_side(arrays, axis, dim, along):
    ends, at = ([], 0)
    for a in arrays[:-1]:
        at += a.shape[along]
        ends.append(at)
    both = jnp.concatenate(arrays, axis=along)
    return tuple(jnp.split(lax.all_gather(both, axis, axis=dim, tiled=True), ends, axis=along))


def sent_to_all(array, axis):
    copies = jnp.broadcast_to(array, (lax.axis_size(axis), *array.shape))
    return lax.all_to_all(copies, axis, split_axis=0, concat_axis=0, tiled=True)


def over_copies(array, axis):
    return sent_to_all(array, axis).sum(axis=0)


def cut_along(array, dim, devices):
    shape = array.shape
    parts = array.reshape(*shape[:dim], devices, shape[dim] // devices, *shape[dim + 1 :])
    return jnp.moveaxis(parts, dim, 0)


def summed_on_arrival(array, axis, dim):
    parts = cut_along(array, dim, lax.axis_size(axis))
    arrived = lax.all_to_all(parts, axis, split_axis=0, concat_axis=0, tiled=True)
    return arrived.astype(jnp.float32).sum(axis=0)


def laid_out(parts, dim):
    shape = list(parts.shape[1:])
    shape[dim] *= parts.shape[0]
    return jnp.moveaxis(parts, 0, dim).reshape(shape)


def gather_directly(array, axis, dim):
    parts = sent_to_all(array, axis)
    return laid_out(parts, dim)


def rotate(values, places):
    half = values.shape[-1] // 2
    inverse = THETA ** (-jnp.arange(half, dtype=jnp.float32) / half)
    angle = places[..., None] * inverse
    cosine = jnp.cos(angle)
    sine = jnp.sin(angle)
    first = values[..., :half]
    second = values[..., half:]
    return jnp.concatenate(
        [first * cosine - second * sine, first * sine + second * cosine], axis=-1
    )


def norm_rows(values, gain):
    wide = values.astype(jnp.float32)
    return wide * lax.rsqrt(jnp.mean(wide * wide, axis=-1, keepdims=True) + EPSILON) * gain


def make_keys(latent_piece, rotary_piece, start, lat_gain, kv_weight):
    normed = norm_rows(latent_piece, lat_gain).astype(jnp.bfloat16)
    key_value = jnp.dot(normed, kv_weight, preferred_element_type=jnp.float32).astype(jnp.bfloat16)
    key_index = start + jnp.arange(latent_piece.shape[0], dtype=jnp.int32)
    key_rope = rotate(rotary_piece.astype(jnp.float32), key_index.astype(jnp.float32)).astype(
        jnp.bfloat16
    )
    return (key_value, key_rope)


def body(
    resid,
    queries,
    latent,
    rope_key,
    lat_gain,
    kv_weight,
    out_gain,
    out_weight,
    ffn_gain,
    gate_weight,
    up_weight,
    down_weight,
):
    rows_here = resid.shape[0]
    first_row = lax.axis_index("sp") * rows_here
    heads_here = queries.shape[1] // (NOPE + ROPE)
    whole_gate, whole_up, whole_down = turned_gather(
        (gate_weight, up_weight, down_weight), "sp", (0, 0, 1)
    )
    query = queries.reshape(rows_here, heads_here, NOPE + ROPE)
    query_index = first_row + jnp.arange(rows_here, dtype=jnp.int32)
    query_nope = query[:, :, :NOPE]
    query_rope = rotate(
        query[:, :, NOPE:].astype(jnp.float32), query_index.astype(jnp.float32)[:, None]
    ).astype(jnp.bfloat16)
    scale = 1.0 / math.sqrt(NOPE + ROPE)

    def accumulate(state, key_value, key_rope):
        running_max, running_sum, weighted = state
        length = key_value.shape[0]
        key_value = key_value.reshape(length, heads_here, NOPE + VDIM)
        key_index = jnp.arange(length, dtype=jnp.int32)
        scores = jnp.einsum(
            "qhd,khd->hqk", query_nope, key_value[:, :, :NOPE], preferred_element_type=jnp.float32
        )
        scores = (
            scores
            + jnp.einsum("qhr,kr->hqk", query_rope, key_rope, preferred_element_type=jnp.float32)
        ) * scale
        allowed = (key_index[None, :] <= query_index[:, None])[None]
        scores = jnp.where(allowed, scores, LOWEST)
        new_max = jnp.maximum(running_max, jnp.max(scores, axis=-1))
        weights = jnp.where(allowed, jnp.exp(scores - new_max[:, :, None]), 0.0)
        running_sum = jnp.sum(weights, axis=-1)
        added = jnp.einsum(
            "hqk,khd->qhd",
            weights.astype(jnp.bfloat16),
            key_value[:, :, NOPE:],
            preferred_element_type=jnp.float32,
        )
        weighted = added
        return (new_max, running_sum, weighted)

    def unchanged(state):
        return state

    initial = (
        jnp.full((heads_here, rows_here), LOWEST, jnp.float32),
        jnp.zeros((heads_here, rows_here), jnp.float32),
        jnp.zeros((rows_here, heads_here, VDIM), jnp.float32),
    )
    own_value, own_rope = make_keys(latent, rope_key, first_row, lat_gain, kv_weight)
    pieces = side_by_side((own_value, own_rope), "sp", 0, 1)

    def update(state):
        return accumulate(state, pieces[0], pieces[1])

    running_max, running_sum, weighted = lax.cond(
        jnp.int32(0) < first_row + rows_here, update, unchanged, initial
    )
    attended = (weighted / jnp.transpose(running_sum)[:, :, None]).astype(jnp.bfloat16)
    attended_float = attended.reshape(rows_here, heads_here * VDIM).astype(jnp.float32)
    squares = over_copies(jnp.sum(attended_float * attended_float, axis=1), "tp")
    normed_out = attended_float * lax.rsqrt(squares / (HEADS * VDIM) + EPSILON)[:, None] * out_gain
    normed_out = normed_out.astype(jnp.bfloat16)
    share = rows_here // lax.axis_size("tp")
    own_first = lax.axis_index("tp") * share
    attn_sum = summed_on_arrival(
        jnp.dot(normed_out, out_weight, preferred_element_type=jnp.float32).astype(jnp.bfloat16),
        "tp",
        0,
    )
    own_resid = lax.dynamic_slice_in_dim(resid, own_first, share, 0)
    middle = (own_resid.astype(jnp.float32) + attn_sum).astype(jnp.bfloat16)
    normed_mid = gather_directly(norm_rows(middle, ffn_gain).astype(jnp.bfloat16), "tp", 0)
    gate = jnp.dot(normed_mid, whole_gate, preferred_element_type=jnp.float32)
    upward = jnp.dot(normed_mid, whole_up, preferred_element_type=jnp.float32)
    hidden = (jax.nn.silu(gate) * upward).astype(jnp.bfloat16)
    terms = jnp.dot(hidden, whole_down, preferred_element_type=jnp.float32)
    ffn_sum = summed_on_arrival(terms.astype(jnp.bfloat16), "tp", 0)
    return (middle.astype(jnp.float32) + ffn_sum).astype(jnp.bfloat16)


def solution(mesh):
    placed = (
        P("sp", None),
        P("sp", "tp"),
        P("sp", None),
        P("sp", None),
        P(),
        P(None, "tp"),
        P("tp"),
        P("tp", None),
        P(),
        P("sp", "tp"),
        P("sp", "tp"),
        P("tp", "sp"),
    )
    return jax.shard_map(
        body, mesh=mesh, in_specs=placed, out_specs=P(("sp", "tp"), None), check_vma=False
    )
```

profile of v0, /device:TPU:1, one launch (start us, length us, event | category | flops | bytes accessed | tf_op | source)
XLA Modules:
  0.0 339.7 jit_solution(4206966190794154403)
XLA Ops:
  6.5 0.0 copy-start
  6.5 0.0 all-gather.3.cloned.1.call-start
  6.6 0.9 convert_element_type.86
  7.5 0.2 multiply_cosine_fusion
  7.7 0.1 copy.62
  7.8 0.1 copy.63
  7.9 1.1 fusion.41
  9.0 1.5 convolution_convert_fusion.1
  10.5 0.8 pad_maximum_fusion.1
  11.4 0.0 all-gather.3.cloned.1.call-update
  11.4 0.0 all-gather.5.cloned.1.call-start
  11.4 1.1 copy.68
  12.5 1.1 copy.69
  13.6 1.8 pad_maximum_fusion
  15.4 0.0 all-gather.5.cloned.1.call-update
  15.4 1.1 copy.61
  16.6 106.4 %all-gather.3.cloned.1.call-done = bf16[8192,576]{1,0:T(8,128)(2,1)} async-done(((bf16[256,576]{1,0:T(8,128)(2,1)}), bf16[8192,576]{1,0:T(8,128)(2,1)}) %all-gather.3.cloned.1.call-update) | async-done | bytes 9437200 | tf_op jit(solution)/shard_map/all_gather | solution.py:33
  123.0 0.0 copy-start.3
  123.0 65.7 %conditional.1 = (f32[2,256]{1,0:T(2,128)S(1)}, f32[256,2,128]{0,2,1:T(8,128)S(1)}) conditional(s32[]{:T(128)} %convert_element_type.82, () %tuple.13, (s32[]{:T(128)}, s32[256]{0:T(256)S(1)}, bf16[256,2,192]{0,2,1:T(8,128)(2,1)S(1)}, bf16[8192,576]{1,0:T(8,128)(2,1)}, bf16[256,2,64]{0,2,1:T(8,128)(2,1)S(1)}) %tuple.36), branch_computations={%region_1.0_spmd, %region_2.5_spmd} | conditional | flops 2728394496 | bytes 147143728 | solution.py:164
  123.0 13.1 %copy.65 = bf16[8192,576]{0,1:T(8,128)(2,1)} copy(bf16[8192,576]{1,0:T(8,128)(2,1)} %get-tuple-element.53) | data formatting | bytes 18874368 | tf_op jit(solution)/shard_map
  136.1 7.9 %split.8 = bf16[8192,512]{0,1:T(8,128)(2,1)} slice(bf16[8192,576]{0,1:T(8,128)(2,1)} %copy.65), slice={[0:8192], [0:512]} | slice | bytes 16777216 | tf_op jit(solution)/shard_map/split | solution.py:33
  144.0 2.6 iota_compare_fusion
  146.6 9.4 %fusion.16 = f32[8192,256,2]{0,1,2:T(8,128)} fusion(bf16[256,2,64]{0,2,1:T(8,128)(2,1)S(1)} %get-tuple-element.25, bf16[8192,576]{0,1:T(8,128)(2,1)} %copy.65), kind=kOutput, calls=%fused_computation.15 | convolution fusion | flops 536870912 | bytes 17891328 | tf_op jit(solution)/shard_map/cond/branch_1_fun/qhr,kr->hqk/dot_general | solution.py:134
  156.0 0.1 copy.64
  156.2 0.0 copy-start.1
  156.2 15.2 %fusion.57 = (f32[2,256]{1,0:T(2,128)S(1)}, f32[2,256,8192]{2,1,0:T(8,128)}) fusion(f32[8192,256,2]{0,1,2:T(8,128)} %fusion.16, bf16[8192,2,256]{0,2,1:T(8,128)(2,1)} %bitcast.30, bf16[256,2,192]{2,0,1:T(8,128)(2,1)S(1)} %copy.64, pred[256,8192]{1,0:T(8,128)(4,1)} %iota_compare_fusion), kind=kOutput, calls=%fused_computation.76 | convolution fusion | flops 1090518528 | bytes 39979008 | tf_op jit(solution)/shard_map/cond/branch_1_fun/qhd,khd->hqk/dot_general | solution.py:129
  171.3 0.0 copy-done.1
  171.3 8.6 %fusion.11 = f32[256,2,128]{2,0,1:T(8,128)S(1)} fusion(bf16[8192,2,256]{0,2,1:T(8,128)(2,1)} %bitcast.31, f32[2,256,8192]{2,1,0:T(8,128)} %get-tuple-element.61, f32[2,256]{1,0:T(2,128)S(1)} %broadcast_maximum_fusion, pred[256,8192]{1,0:T(8,128)(4,1)S(1)} %copy-done.1), kind=kOutput, calls=%fused_computation.13 | convolution fusion | flops 1086324736 | bytes 23332864 | tf_op jit(solution)/shard_map/cond/branch_1_fun/hqk,khd->qhd/dot_general | solution.py:141
  180.0 0.1 copy.72
  180.1 8.5 %fusion.3 = f32[2,256]{1,0:T(2,128)S(1)} fusion(f32[2,256,8192]{2,1,0:T(8,128)} %get-tuple-element.61, f32[2,256]{1,0:T(2,128)S(1)} %broadcast_maximum_fusion, pred[256,8192]{1,0:T(8,128)(4,1)} %iota_compare_fusion), kind=kLoop, calls=%fused_computation.5 | loop fusion | flops 12582400 | bytes 18878464 | tf_op jit(solution)/shard_map/cond/branch_1_fun/reduce_sum | solution.py:140
  188.6 0.1 multiply_reduce_fusion
  188.7 10.3 %all_to_all.21 = f32[8,1,256]{2,1,0:T(1,128)S(1)} all-to-all(f32[8,1,256]{2,1,0:T(1,128)S(1)} %broadcast_in_dim.47), channel_id=1, replica_groups=mesh['sp'=32,'tp'=8] {'tp'}, dimensions={0} | all-to-all | bytes 16384 | tf_op jit(solution)/shard_map/all_to_all | solution.py:38
  199.1 0.0 copy-done.3
  199.1 0.0 copy-start.2
  199.1 0.1 fusion.51
  199.2 0.0 copy-done
  199.2 2.1 convolution_convert_fusion
  201.3 4.9 %all-to-all-start.1 = ((bf16[8,32,4096]{2,1,0:T(8,128)(2,1)}), bf16[8,32,4096]{2,1,0:T(8,128)(2,1)}, u32[]{:S(2)}, u32[]{:S(2)}) async-start(bf16[8,32,4096]{2,1,0:T(8,128)(2,1)} %bitcast.32), calls=%async_computation.1 | async-start | bytes 4194304 | tf_op jit(solution)/shard_map/all_to_all | solution.py:53
  206.1 26.3 %all-to-all-done.1 = bf16[8,32,4096]{2,1,0:T(8,128)(2,1)} async-done(((bf16[8,32,4096]{2,1,0:T(8,128)(2,1)}), bf16[8,32,4096]{2,1,0:T(8,128)(2,1)}, u32[]{:S(2)}, u32[]{:S(2)}) %all-to-all-start.1) | async-done | bytes 2097184 | tf_op jit(solution)/shard_map/all_to_all | solution.py:53
  232.5 2.0 convert_reduce_fusion.1
  234.5 1.2 fusion.44
  235.6 0.0 copy-done.2
  235.6 0.1 fusion.46
  235.8 0.2 broadcast_in_dim.48
  236.0 30.3 %all_to_all.22 = bf16[8,32,4096]{2,1,0:T(8,128)(2,1)} all-to-all(bf16[8,32,4096]{2,1,0:T(8,128)(2,1)S(1)} %broadcast_in_dim.48), channel_id=1, replica_groups=mesh['sp'=32,'tp'=8] {'tp'}, dimensions={0} | all-to-all | bytes 4194304 | tf_op jit(solution)/shard_map/all_to_all | solution.py:38
  266.3 14.7 %all-gather.5.cloned.1.call-done = bf16[4096,2304]{0,1:T(8,128)(2,1)} async-done(((bf16[128,2304]{0,1:T(8,128)(2,1)}), bf16[4096,2304]{0,1:T(8,128)(2,1)}) %all-gather.5.cloned.1.call-update) | async-done | bytes 18874384 | tf_op jit(solution)/shard_map/all_gather | solution.py:19
  281.0 5.2 %fusion.23 = f32[256,768]{1,0:T(8,128)S(1)} fusion(bf16[256,4096]{1,0:T(8,128)(2,1)} %bitcast.33, bf16[4096,2304]{0,1:T(8,128)(2,1)} %all-gather.5.cloned.1.call-done), kind=kOutput, calls=%fused_computation.24 | convolution fusion | flops 1610612736 | bytes 9175040 | tf_op jit(solution)/shard_map/dot_general | solution.py:182
  286.2 11.1 %fusion.25 = bf16[256,4096]{1,0:T(8,128)(2,1)} fusion(bf16[4096,2304]{0,1:T(8,128)(2,1)} %all-gather.5.cloned.1.call-done, bf16[256,4096]{1,0:T(8,128)(2,1)} %bitcast.34, f32[256,768]{1,0:T(8,128)S(1)} %fusion.23), kind=kOutput, calls=%fused_computation.27 | convolution fusion | flops 3223453696 | bytes 17563648 | tf_op jit(solution)/shard_map/dot_general | solution.py:185
  297.3 34.5 %all_to_all.23 = bf16[8,32,4096]{2,1,0:T(8,128)(2,1)S(1)} all-to-all(bf16[8,32,4096]{2,1,0:T(8,128)(2,1)} %bitcast.35), channel_id=1, replica_groups=mesh['sp'=32,'tp'=8] {'tp'}, dimensions={0} | all-to-all | bytes 4194304 | tf_op jit(solution)/shard_map/all_to_all | solution.py:53
  331.8 0.3 convert_reduce_fusion
  332.1 0.8 fusion.47
  (13 shorter events, 0.1 us)
Async XLA Ops:
  6.5 192.7 %copy-start = (bf16[256,4096]{1,0:T(8,128)(2,1)S(1)}, bf16[256,4096]{1,0:T(8,128)(2,1)}, u32[]{:S(2)}) copy-start(bf16[256,4096]{1,0:T(8,128)(2,1)} %param.21) | copy-start | bytes 6291460
  6.5 116.4 %all-gather.3.cloned.1.call-start = ((), (), s32[]{:S(2)}) async-start(), calls=%async_computation.4 | async-start | bytes 10813440 | tf_op jit(solution)/shard_map/all_gather | solution.py:33
  11.4 269.6 %all-gather.5.cloned.1.call-start = ((), (), s32[]{:S(2)}) async-start(), calls=%async_computation.5 | async-start | bytes 19464192 | tf_op jit(solution)/shard_map/all_gather | solution.py:19
  123.0 76.1 %copy-start.3 = (f32[256]{0:T(256)S(1)}, f32[256]{0:T(256)}, u32[]{:S(2)}) copy-start(f32[256]{0:T(256)} %param.20) | copy-start | bytes 3076
  156.2 15.2 %copy-start.1 = (pred[256,8192]{1,0:T(8,128)(4,1)S(1)}, pred[256,8192]{1,0:T(8,128)(4,1)}, u32[]{:S(2)}) copy-start(pred[256,8192]{1,0:T(8,128)(4,1)} %iota_compare_fusion) | copy-start | bytes 6291460 | tf_op jit(solution)/shard_map/cond
  199.1 36.5 %copy-start.2 = (f32[4096]{0:T(1024)S(1)}, f32[4096]{0:T(1024)}, u32[]{:S(2)}) copy-start(f32[4096]{0:T(1024)} %param.22) | copy-start | bytes 49156
  201.3 31.2 %all-to-all-start.1 = ((bf16[8,32,4096]{2,1,0:T(8,128)(2,1)}), bf16[8,32,4096]{2,1,0:T(8,128)(2,1)}, u32[]{:S(2)}, u32[]{:S(2)}) async-start(bf16[8,32,4096]{2,1,0:T(8,128)(2,1)} %bitcast.32), calls=%async_computation.1 | async-start | bytes 4194304 | tf_op jit(solution)/shard_map/all_to_all | solution.py:53
Sparse Core Ops, SparseCore 0:
  11.5 111.4 all-gather.2
  125.4 155.4 all-gather.4
where the time goes:
time: 341 us; the launch traced here: 340 us
  waiting for transfers between devices  147 us (43%)
  blocking collectives  75.1 us (22%)
  matrix products  53.1 us (16%)
  local copies, waits for them, and re-layouts  25 us (7%)
  other arithmetic  20.6 us (6%)
  between operations  13.5 us (4%)
  starting transfers between devices  4.9 us (1%)
    all_gather x1, waiting for transfers between devices, side_by_side(): lax.all_gather(both, axis, axis=dim, tiled=True)  106 us
    all_to_all x2, blocking collectives, sent_to_all(): return lax.all_to_all(copies, axis, split_axis=0, concat_axis=0, tiled=True)  40.6 us
    all_to_all x1, blocking collectives, summed_on_arrival(): lax.all_to_all(parts, axis, split_axis=0, concat_axis=0, tiled=True)  34.5 us
    all_to_all x1, waiting for transfers between devices, summed_on_arrival(): lax.all_to_all(parts, axis, split_axis=0, concat_axis=0, tiled=True)  26.3 us
    dot_general x1, matrix products, accumulate(): jnp.einsum('qhd,khd->hqk', query_nope, key_value[:, :, :NOPE], preferred_...  15.2 us
    all_gather x1, waiting for transfers between devices, turned_gather(): filled, at, outs = (lax.all_gather(both, axis, axis=0, tiled=True), 0, [])  14.7 us
    another operation x4, local copies, waits for them, and re-layouts  13.5 us
    dot_general x1, matrix products, body(): terms = jnp.dot(hidden, whole_down, preferred_element_type=jnp.float32)  11.1 us
  transfers between devices with their start and end apart: 3, of which 3 were waited for; matrix products, arithmetic and copies ran while one was open for 23% of the time, Pallas kernels for 0%

commit v1 on v0

--- a/solution.py
+++ b/solution.py
@@ -16,7 +16,13 @@
 def turned_gather(arrays, axis, dims):
     turned = [jnp.moveaxis(a, dim, 0) for a, dim in zip(arrays, dims)]
     both = jnp.concatenate([t.reshape(len(t), -1) for t in turned], axis=1)
-    filled, at, outs = (lax.all_gather(both, axis, axis=0, tiled=True), 0, [])
+    filled, at, outs = (
+        jnp.concatenate(
+            lax.all_to_all(jnp.stack([both] * lax.axis_size(axis)), axis, 0, 0), axis=0
+        ),
+        0,
+        [],
+    )
     for t, dim in zip(turned, dims):
         slab = filled[:, at : at + t[0].size].reshape(-1, *t.shape[1:])
         outs.append(jnp.moveaxis(slab, 0, dim))

time: 341 us -> 743 us (2.18)
  blocking collectives: 75.1 us -> 456 us
  waiting for transfers between devices: 147 us -> 162 us
  local copies, waits for them, and re-layouts: 25 us -> 33.2 us
    all_to_all x0 -> x1, blocking collectives: none -> 413 us  [turned_gather(): lax.all_to_all(jnp.stack([both] * lax.axis_size(axis)), axis, 0, 0)]
    all_to_all x2 -> x1, blocking collectives: 40.6 us -> 10.1 us  [sent_to_all(): return lax.all_to_all(copies, axis, split_axis=0, concat_axis=0, tiled=True)]
    all_to_all x0 -> x1, waiting for transfers between devices: none -> 25.7 us  [sent_to_all(): return lax.all_to_all(copies, axis, split_axis=0, concat_axis=0, tiled=True)]
    all_gather x1 -> x0, waiting for transfers between devices: 14.7 us -> none  [turned_gather(): filled, at, outs = (lax.all_gather(both, axis, axis=0, tiled=True), 0, [])]
    another operation x4 -> x5, local copies, waits for them, and re-layouts: 13.5 us -> 15.7 us
  transfers between devices with their start and end apart: 3 -> 3, of which waited for: 3 -> 3; matrix products, arithmetic and copies ran while one was open for 23% -> 0% of each run, Pallas kernels for 0% -> 0%
where the time goes in v1:
time: 743 us
  blocking collectives  456 us (61%)
  waiting for transfers between devices  162 us (22%)
  matrix products  51.1 us (7%)
  local copies, waits for them, and re-layouts  33.2 us (4%)
  other arithmetic  16.9 us (2%)
  between operations  13.6 us (2%)
  starting transfers between devices  9.41 us (1%)
    all_to_all x1, blocking collectives, turned_gather(): lax.all_to_all(jnp.stack([both] * lax.axis_size(axis)), axis, 0, 0)  413 us
    all_gather x1, waiting for transfers between devices, side_by_side(): lax.all_gather(both, axis, axis=dim, tiled=True)  110 us
    all_to_all x1, blocking collectives, summed_on_arrival(): lax.all_to_all(parts, axis, split_axis=0, concat_axis=0, tiled=True)  32.6 us
    all_to_all x1, waiting for transfers between devices, summed_on_arrival(): lax.all_to_all(parts, axis, split_axis=0, concat_axis=0, tiled=True)  26.2 us
    all_to_all x1, waiting for transfers between devices, sent_to_all(): return lax.all_to_all(copies, axis, split_axis=0, concat_axis=0, tiled=True)  25.7 us
    dot_general x1, matrix products, accumulate(): jnp.einsum('qhd,khd->hqk', query_nope, key_value[:, :, :NOPE], preferred_...  14.9 us
  transfers between devices with their start and end apart: 3, of which 3 were waited for; matrix products, arithmetic and copies ran while one was open for 0% of the time, Pallas kernels for 0%

profile of v1, /device:TPU:1, one launch (start us, length us, event | category | flops | bytes accessed | tf_op | source)
XLA Modules:
  0.0 742.5 jit_solution(13898491181106861653)
XLA Ops:
  6.5 0.0 copy-start
  6.5 0.0 all-gather.2.cloned.1.call-start
  6.6 0.9 convert_element_type.86
  7.5 0.2 multiply_cosine_fusion
  7.7 0.1 copy.66
  7.8 0.1 copy.67
  7.9 1.1 fusion.41
  9.0 1.5 convolution_convert_fusion.1
  10.5 0.8 pad_maximum_fusion.1
  11.3 0.0 all-gather.2.cloned.1.call-update
  11.3 1.1 copy.65
  12.5 110.5 %all-gather.2.cloned.1.call-done = bf16[8192,576]{1,0:T(8,128)(2,1)} async-done(((bf16[256,576]{1,0:T(8,128)(2,1)}), bf16[8192,576]{1,0:T(8,128)(2,1)}) %all-gather.2.cloned.1.call-update) | async-done | bytes 9437200 | tf_op jit(solution)/shard_map/all_gather | solution.py:39
  122.9 0.0 copy-start.8
  122.9 64.9 %conditional.1 = (f32[2,256]{1,0:T(2,128)S(1)}, f32[256,2,128]{0,2,1:T(8,128)S(1)}) conditional(s32[]{:T(128)} %convert_element_type.82, () %tuple.13, (s32[]{:T(128)}, s32[256]{0:T(256)S(1)}, bf16[256,2,192]{0,2,1:T(8,128)(2,1)S(1)}, bf16[8192,576]{1,0:T(8,128)(2,1)}, bf16[256,2,64]{0,2,1:T(8,128)(2,1)S(1)}) %tuple.34), branch_computations={%region_1.0_spmd, %region_2.5_spmd} | conditional | flops 2728394496 | bytes 147143728 | solution.py:170
  122.9 13.1 %copy.69 = bf16[8192,576]{0,1:T(8,128)(2,1)} copy(bf16[8192,576]{1,0:T(8,128)(2,1)} %get-tuple-element.53) | data formatting | bytes 18874368 | tf_op jit(solution)/shard_map
  136.1 7.7 %split.8 = bf16[8192,512]{0,1:T(8,128)(2,1)} slice(bf16[8192,576]{0,1:T(8,128)(2,1)} %copy.69), slice={[0:8192], [0:512]} | slice | bytes 16777216 | tf_op jit(solution)/shard_map/split | solution.py:39
  143.8 2.7 iota_compare_fusion
  146.4 9.3 %fusion.16 = f32[8192,256,2]{0,1,2:T(8,128)} fusion(bf16[256,2,64]{0,2,1:T(8,128)(2,1)S(1)} %get-tuple-element.25, bf16[8192,576]{0,1:T(8,128)(2,1)} %copy.69), kind=kOutput, calls=%fused_computation.15 | convolution fusion | flops 536870912 | bytes 17891328 | tf_op jit(solution)/shard_map/cond/branch_1_fun/qhr,kr->hqk/dot_general | solution.py:140
  155.7 0.1 copy.68
  155.9 0.0 copy-start.2
  155.9 14.9 %fusion.57 = (f32[2,256]{1,0:T(2,128)S(1)}, f32[2,256,8192]{2,1,0:T(8,128)}) fusion(f32[8192,256,2]{0,1,2:T(8,128)} %fusion.16, bf16[8192,2,256]{0,2,1:T(8,128)(2,1)} %bitcast.33, bf16[256,2,192]{2,0,1:T(8,128)(2,1)S(1)} %copy.68, pred[256,8192]{1,0:T(8,128)(4,1)} %iota_compare_fusion), kind=kOutput, calls=%fused_computation.76 | convolution fusion | flops 1090518528 | bytes 39979008 | tf_op jit(solution)/shard_map/cond/branch_1_fun/qhd,khd->hqk/dot_general | solution.py:135
  170.8 0.0 copy-done.2
  170.8 8.6 %fusion.11 = f32[256,2,128]{2,0,1:T(8,128)S(1)} fusion(bf16[8192,2,256]{0,2,1:T(8,128)(2,1)} %bitcast.34, f32[2,256,8192]{2,1,0:T(8,128)} %get-tuple-element.61, f32[2,256]{1,0:T(2,128)S(1)} %broadcast_maximum_fusion, pred[256,8192]{1,0:T(8,128)(4,1)S(1)} %copy-done.2), kind=kOutput, calls=%fused_computation.13 | convolution fusion | flops 1086324736 | bytes 23332864 | tf_op jit(solution)/shard_map/cond/branch_1_fun/hqk,khd->qhd/dot_general | solution.py:147
  179.5 0.1 copy.77
  179.6 8.3 %fusion.3 = f32[2,256]{1,0:T(2,128)S(1)} fusion(f32[2,256,8192]{2,1,0:T(8,128)} %get-tuple-element.61, f32[2,256]{1,0:T(2,128)S(1)} %broadcast_maximum_fusion, pred[256,8192]{1,0:T(8,128)(4,1)} %iota_compare_fusion), kind=kLoop, calls=%fused_computation.5 | loop fusion | flops 12582400 | bytes 18878464 | tf_op jit(solution)/shard_map/cond/branch_1_fun/reduce_sum | solution.py:146
  187.9 0.1 multiply_reduce_fusion
  188.0 10.1 %all_to_all.26 = f32[8,1,256]{2,1,0:T(1,128)S(1)} all-to-all(f32[8,1,256]{2,1,0:T(1,128)S(1)} %broadcast_in_dim.47), channel_id=1, replica_groups=mesh['sp'=32,'tp'=8] {'tp'}, dimensions={0} | all-to-all | bytes 16384 | tf_op jit(solution)/shard_map/all_to_all | solution.py:44
  198.1 0.0 copy-done.8
  198.1 0.0 copy-start.7
  198.1 0.1 fusion.51
  198.2 0.0 copy-done
  198.2 2.1 convolution_convert_fusion
  200.3 4.2 all-to-all-start.1
  204.5 0.0 copy-start.5
  204.5 0.0 copy-start.6
  204.5 0.0 copy-start.4
  204.5 26.2 %all-to-all-done.1 = bf16[8,32,4096]{2,1,0:T(8,128)(2,1)S(1)} async-done(((bf16[8,32,4096]{2,1,0:T(8,128)(2,1)}), bf16[8,32,4096]{2,1,0:T(8,128)(2,1)S(1)}, u32[]{:S(2)}, u32[]{:S(2)}) %all-to-all-start.1) | async-done | bytes 2097184 | tf_op jit(solution)/shard_map/all_to_all | solution.py:59
  230.8 0.3 convert_reduce_fusion.1
  231.1 1.1 fusion.44
  232.2 0.0 copy-done.7
  232.2 0.1 fusion.46
  232.4 1.6 broadcast_in_dim.48
  233.9 5.2 all-to-all-start.2
  239.1 0.0 copy-done.5
  239.2 0.2 copy.72
  239.3 0.0 copy-done.6
  239.3 0.2 copy.73
  239.5 0.0 copy-done.4
  239.5 0.2 copy.74
  239.8 25.7 %all-to-all-done.2 = bf16[8,32,4096]{2,1,0:T(8,128)(2,1)} async-done(((bf16[8,32,4096]{2,1,0:T(8,128)(2,1)}), bf16[8,32,4096]{2,1,0:T(8,128)(2,1)}, u32[]{:S(2)}, u32[]{:S(2)}) %all-to-all-start.2) | async-done | bytes 2097184 | tf_op jit(solution)/shard_map/all_to_all | solution.py:44
  265.5 2.2 stack.2
  267.7 413.2 %all_to_all.27 = bf16[32,128,2304]{2,1,0:T(8,128)(2,1)S(1)} all-to-all(bf16[32,128,2304]{2,1,0:T(8,128)(2,1)S(1)} %stack.2), channel_id=1, replica_groups=mesh['sp'=32,'tp'=8] {'sp'}, dimensions={0} | all-to-all | bytes 37748736 | tf_op jit(solution)/shard_map/all_to_all | solution.py:21
  680.9 0.0 copy-start.3
  680.9 6.5 copy-done.3
  687.3 3.4 fusion.23
  690.7 0.0 copy-start.1
  690.8 11.2 %fusion.25 = bf16[256,4096]{1,0:T(8,128)(2,1)} fusion(bf16[4096,2304]{1,0:T(8,128)(2,1)} %bitcast.32, bf16[256,4096]{1,0:T(8,128)(2,1)} %bitcast.8, f32[256,768]{1,0:T(8,128)S(1)} %fusion.23), kind=kOutput, calls=%fused_computation.27 | convolution fusion | flops 3223453696 | bytes 17563648 | tf_op jit(solution)/shard_map/dot_general | solution.py:191
  702.0 32.6 %all_to_all.28 = bf16[8,32,4096]{2,1,0:T(8,128)(2,1)S(1)} all-to-all(bf16[8,32,4096]{2,1,0:T(8,128)(2,1)} %bitcast.36), channel_id=1, replica_groups=mesh['sp'=32,'tp'=8] {'tp'}, dimensions={0} | all-to-all | bytes 4194304 | tf_op jit(solution)/shard_map/all_to_all | solution.py:59
  734.6 0.3 convert_reduce_fusion
  734.9 0.8 fusion.47
  735.7 0.0 copy-done.1
  (14 shorter events, 0.2 us)
Async XLA Ops:
  6.5 191.7 %copy-start = (bf16[256,4096]{1,0:T(8,128)(2,1)S(1)}, bf16[256,4096]{1,0:T(8,128)(2,1)}, u32[]{:S(2)}) copy-start(bf16[256,4096]{1,0:T(8,128)(2,1)} %param.21) | copy-start | bytes 6291460
  6.5 116.4 %all-gather.2.cloned.1.call-start = ((), (), s32[]{:S(2)}) async-start(), calls=%async_computation.5 | async-start | bytes 10813440 | tf_op jit(solution)/shard_map/all_gather | solution.py:39
  122.9 75.2 %copy-start.8 = (f32[256]{0:T(256)S(1)}, f32[256]{0:T(256)}, u32[]{:S(2)}) copy-start(f32[256]{0:T(256)} %param.20) | copy-start | bytes 3076
  155.9 15.0 %copy-start.2 = (pred[256,8192]{1,0:T(8,128)(4,1)S(1)}, pred[256,8192]{1,0:T(8,128)(4,1)}, u32[]{:S(2)}) copy-start(pred[256,8192]{1,0:T(8,128)(4,1)} %iota_compare_fusion) | copy-start | bytes 6291460 | tf_op jit(solution)/shard_map/cond
  198.1 34.1 %copy-start.7 = (f32[4096]{0:T(1024)S(1)}, f32[4096]{0:T(1024)}, u32[]{:S(2)}) copy-start(f32[4096]{0:T(1024)} %param.22) | copy-start | bytes 49156
  200.3 30.4 %all-to-all-start.1 = ((bf16[8,32,4096]{2,1,0:T(8,128)(2,1)}), bf16[8,32,4096]{2,1,0:T(8,128)(2,1)S(1)}, u32[]{:S(2)}, u32[]{:S(2)}) async-start(bf16[8,32,4096]{2,1,0:T(8,128)(2,1)} %bitcast.35), calls=%async_computation.1 | async-start | bytes 4194304 | tf_op jit(solution)/shard_map/all_to_all | solution.py:59
  204.5 34.6 %copy-start.5 = (bf16[128,768]{1,0:T(8,128)(2,1)S(1)}, bf16[128,768]{1,0:T(8,128)(2,1)}, u32[]{:S(2)}) copy-start(bf16[128,768]{1,0:T(8,128)(2,1)} %param.23) | copy-start | bytes 589828
  204.5 34.8 %copy-start.6 = (bf16[128,768]{1,0:T(8,128)(2,1)S(1)}, bf16[128,768]{1,0:T(8,128)(2,1)}, u32[]{:S(2)}) copy-start(bf16[128,768]{1,0:T(8,128)(2,1)} %param.24) | copy-start | bytes 589828
  204.5 35.0 %copy-start.4 = (bf16[768,128]{1,0:T(8,128)(2,1)S(1)}, bf16[768,128]{1,0:T(8,128)(2,1)}, u32[]{:S(2)}) copy-start(bf16[768,128]{1,0:T(8,128)(2,1)} %param.25) | copy-start | bytes 589828
  233.9 31.5 %all-to-all-start.2 = ((bf16[8,32,4096]{2,1,0:T(8,128)(2,1)}), bf16[8,32,4096]{2,1,0:T(8,128)(2,1)}, u32[]{:S(2)}, u32[]{:S(2)}) async-start(bf16[8,32,4096]{2,1,0:T(8,128)(2,1)} %broadcast_in_dim.48), calls=%async_computation.2 | async-start | bytes 4194304 | tf_op jit(solution)/shard_map/all_to_all | solution.py:44
  680.9 6.5 copy-start.3
  690.7 44.9 %copy-start.1 = (bf16[256,4096]{1,0:T(8,128)(2,1)S(1)}, bf16[256,4096]{1,0:T(8,128)(2,1)}, u32[]{:S(2)}) copy-start(bf16[256,4096]{1,0:T(8,128)(2,1)} %param.21) | copy-start | bytes 6291460
Sparse Core Ops, SparseCore 0:
  11.5 111.4 all-gather.1
